TPU v7x, 32 devices: a whole 2x2x4 slice. The times are simulated.
32 devices in a mesh: fs: 8 (over z, x), tp: 4 (over y, core).
Axes of the slice: x: 2, y: 2, z: 4, core: 2. Of those that a mesh axis runs over, the one named last changes fastest.
Arguments:
- tokens: bfloat16 [320, 4096], P('fs'), may hold values from -6 to 6
- routes: int32 [320, 2], P('fs'), may hold values from 0 to 3, all different within a row; in each aligned block of 40 rows (0 to 39, 40 to 79, ...) at most 30 rows name the same one
- route_logits: float32 [320, 2], P('fs'), may hold values from -6 to 6
- norm_gain: float32 [4096], P('fs'), may hold values from 0.1 to 1.9
- gate_weight: float32 [4, 4096, 8192], P(None, 'fs', 'tp'), may hold values from -0.09375 to 0.09375
- up_weight: float32 [4, 4096, 8192], P(None, 'fs', 'tp'), may hold values from -0.09375 to 0.09375
- down_weight: float32 [4, 4096, 8192], P(None, 'fs', 'tp'), may hold values from -0.0625 to 0.0625
Outputs:
- mixed: bfloat16 [320, 4096], P('fs', 'tp')
- gate_sampler: bfloat16 [4, 4096, 8192], P('tp', None, 'fs')
- up_sampler: bfloat16 [4, 4096, 8192], P('tp', None, 'fs')
- down_sampler: bfloat16 [4, 4096, 8192], P('tp', None, 'fs')
Inputs may be any that keep to these rules, and one draw needn't show every extreme that they name: `routes`: the 2 experts of a token differ. Within the tokens of one index of fs (aligned blocks of 40 rows) no expert is named by more than 30 tokens.
All inputs are finite; a program needn't handle non-finite values.
Results may differ from a plain program's by a relative error of at most 0.01.
Values may be sent and summed in bfloat16 or wider, within the bound.
A program may use at most 192 MiB of HBM per device.

v0:
```python
import functools

import jax
import jax.numpy as jnp
from jax import lax
from jax.experimental import pallas as pl
from jax.experimental.pallas import tpu as pltpu
from jax.sharding import PartitionSpec as P

VMEM_LIMIT = 40 * 1024 * 1024


MESH = pl.DeviceIdType.MESH


def exchange_kernel(
    fs_count, tp_count, experts, pieces,
    tok_ref, routes_ref, logits_ref, gain_ref, gate_hbm, up_hbm, down_hbm,
    rows_out, weights_out, gate_out, up_out, down_out, rest_out,
    xcol, wown, stage, gate_send, up_send, down_send, rest_send,
    load_sem, send_sem, recv_sem, keep_sem, x_send, x_recv, w_send, w_recv, t_send, t_recv,
    own_sem, rest_sem,
):
    me, my_tp = lax.axis_index("fs"), lax.axis_index("tp")
    spread = fs_count // experts
    own = tok_ref.shape[0]
    width, block = stage.shape[1], stage.shape[2]
    part = xcol.shape[2]
    rows = width // pieces
    barrier = pltpu.get_barrier_semaphore()
    for s in range(1, fs_count):
        pl.semaphore_signal(
            barrier, inc=1, device_id={"fs": lax.rem(me + s, fs_count)}, device_id_type=MESH
        )
    for s in range(1, tp_count):
        pl.semaphore_signal(
            barrier, inc=1, device_id={"tp": lax.rem(my_tp + s, tp_count)}, device_id_type=MESH
        )

    def target(step):
        return lax.rem(me + fs_count // 2 + step, fs_count)

    def load(hbm, step, slot):
        dst = target(step)
        column = pl.multiple_of(lax.rem(dst, spread) * block, block)
        return pltpu.make_async_copy(
            hbm.at[dst // spread, :, pl.ds(column, block)], stage.at[slot], load_sem.at[slot]
        )

    load(gate_hbm, 0, 0).start()

    tok = tok_ref[...].astype(jnp.float32)
    scale = lax.rsqrt(jnp.mean(tok * tok, axis=1, keepdims=True) + 1e-05)
    cols = tok_ref[:, pl.ds(pl.multiple_of(my_tp * part, part), part)].astype(jnp.float32)
    xcol[me] = (cols * scale).astype(jnp.bfloat16)
    first, second = logits_ref[:, 0:1], logits_ref[:, 1:2]
    lanes = lax.broadcasted_iota(jnp.int32, (own, 128), 1)
    wown[...] = jnp.where(
        routes_ref[:, 0:1] == lanes, 1.0 / (1.0 + jnp.exp(second - first)), 0.0
    ) + jnp.where(routes_ref[:, 1:2] == lanes, 1.0 / (1.0 + jnp.exp(first - second)), 0.0)
    pl.semaphore_wait(barrier, fs_count + tp_count - 2)

    def x_copy(dst, sem):
        return pltpu.make_async_remote_copy(
            src_ref=xcol.at[me], dst_ref=xcol.at[me], send_sem=x_send.at[dst],
            recv_sem=x_recv.at[sem], device_id={"fs": dst}, device_id_type=MESH,
        )

    def w_copy(dst, sem):
        return pltpu.make_async_remote_copy(
            src_ref=wown, dst_ref=weights_out.at[me], send_sem=w_send.at[dst],
            recv_sem=w_recv.at[sem], device_id={"fs": dst}, device_id_type=MESH,
        )

    w_keep = pltpu.make_async_copy(wown, weights_out.at[me], own_sem.at[0])
    w_keep.start()
    for s in range(1, fs_count):
        dst = lax.rem(me + s, fs_count)
        x_copy(dst, me).start()
        w_copy(dst, me).start()

    weights_in = (
        (gate_hbm, gate_send, gate_out, True),
        (up_hbm, up_send, up_out, True),
        (down_hbm, down_send, down_out, False),
    )

    def w_send_copy(m, dst):
        _, held, out, _ = weights_in[m]
        return pltpu.make_async_remote_copy(
            src_ref=held.at[dst], dst_ref=out.at[me], send_sem=send_sem.at[m, dst],
            recv_sem=recv_sem.at[m, me], device_id={"fs": dst}, device_id_type=MESH,
        )

    def keep_copy(m):
        _, held, out, _ = weights_in[m]
        return pltpu.make_async_copy(held.at[me], out.at[me], keep_sem.at[m])

    t_copies = []
    for m in range(3):
        hbm, held, out, folded = weights_in[m]

        def body(step, carry, m=m, hbm=hbm, held=held, folded=folded):
            slot = lax.rem(m * fs_count + step, 2)
            dst = target(step)

            @pl.when(step + 1 < fs_count)
            def _():
                load(hbm, step + 1, 1 - slot).start()

            if m < 2:

                @pl.when(step + 1 == fs_count)
                def _():
                    load(weights_in[m + 1][0], 0, 1 - slot).start()

            load(hbm, step, slot).wait()
            if folded:
                held[dst] = (stage[slot] * gain_ref[...]).astype(jnp.bfloat16)
            else:
                held[dst] = stage[slot, :rows].astype(jnp.bfloat16)
                if pieces > 1:
                    rest_send[dst] = stage[slot, rows:].astype(jnp.bfloat16)

            @pl.when(dst == me)
            def _():
                keep_copy(m).start()

            @pl.when(dst != me)
            def _():
                w_send_copy(m, dst).start()

            return carry

        lax.fori_loop(0, fs_count, body, 0)
        if m == 0:
            for s in range(1, fs_count):
                src = lax.rem(me + s, fs_count)
                pltpu.make_async_copy(xcol.at[src], xcol.at[src], x_recv.at[src]).wait()
            for s in range(1, tp_count):
                copy = pltpu.make_async_remote_copy(
                    src_ref=xcol, dst_ref=rows_out.at[my_tp], send_sem=t_send.at[s],
                    recv_sem=t_recv.at[s], device_id={"tp": lax.rem(my_tp + s, tp_count)},
                    device_id_type=MESH,
                )
                copy.start()
                t_copies.append(copy)
            x_keep = pltpu.make_async_copy(xcol, rows_out.at[my_tp], own_sem.at[1])
            x_keep.start()
    if pieces > 1:
        rest_copy = pltpu.make_async_copy(rest_send, rest_out, rest_sem)
        rest_copy.start()
        rest_copy.wait()
    w_keep.wait()
    x_keep.wait()
    for s in range(1, tp_count):
        src = lax.rem(my_tp + tp_count - s, tp_count)
        t_copies[s - 1].wait_send()
        pltpu.make_async_copy(xcol, rows_out.at[src], t_recv.at[s]).wait()
    for s in range(1, fs_count):
        other = lax.rem(me + s, fs_count)
        x_copy(other, me).wait_send()
        w_copy(other, me).wait_send()
        pltpu.make_async_copy(wown, weights_out.at[other], w_recv.at[other]).wait()
    for m in range(3):
        _, held, out, _ = weights_in[m]
        keep_copy(m).wait()

        def finish(s, carry, m=m, held=held, out=out):
            other = lax.rem(me + s, fs_count)
            w_send_copy(m, other).wait_send()
            pltpu.make_async_copy(held.at[other], out.at[other], recv_sem.at[m, other]).wait()
            return carry

        lax.fori_loop(1, fs_count, finish, 0)


def exchange(tokens, routes, logits, gain, gate, up, down, fs_count, tp_count, pieces):
    experts, width, columns = gate.shape
    block = columns // (fs_count // experts)
    rows = width // pieces
    own, model = tokens.shape
    part = model // tp_count
    bf16, dma = jnp.bfloat16, pltpu.SemaphoreType.DMA
    vmem = pl.BlockSpec(memory_space=pltpu.VMEM)
    anywhere = pl.BlockSpec(memory_space=pl.ANY)
    return pl.pallas_call(
        functools.partial(exchange_kernel, fs_count, tp_count, experts, pieces),
        in_specs=[vmem] * 4 + [anywhere] * 3,
        out_specs=[anywhere] * 6,
        out_shape=[
            jax.ShapeDtypeStruct((tp_count, fs_count, own, part), bf16),
            jax.ShapeDtypeStruct((fs_count, own, 128), jnp.float32),
            jax.ShapeDtypeStruct((fs_count, width, block), bf16),
            jax.ShapeDtypeStruct((fs_count, width, block), bf16),
            jax.ShapeDtypeStruct((fs_count, rows, block), bf16),
            jax.ShapeDtypeStruct((fs_count, rows, block), bf16),
        ],
        scratch_shapes=[
            pltpu.VMEM((fs_count, own, part), bf16),
            pltpu.VMEM((own, 128), jnp.float32),
            pltpu.VMEM((2, width, block), jnp.float32),
            pltpu.VMEM((fs_count, width, block), bf16),
            pltpu.VMEM((fs_count, width, block), bf16),
            pltpu.VMEM((fs_count, rows, block), bf16),
            pltpu.VMEM((fs_count, rows, block), bf16),
            dma((2,)), dma((3, fs_count)), dma((3, fs_count)), dma((3,)),
            dma((fs_count,)), dma((fs_count,)), dma((fs_count,)), dma((fs_count,)),
            dma((tp_count,)), dma((tp_count,)), dma((2,)), dma,
        ],
        compiler_params=pltpu.CompilerParams(
            collective_id=0, has_side_effects=True, vmem_limit_bytes=56 * 1024 * 1024
        ),
    )(tokens, routes, logits, gain, gate, up, down)


def reduce_kernel(
    fs_count, tp_count, experts, part_ref, out_ref, first, total, second,
    send1, recv1, send2, recv2, keep_sem,
):
    me, my_tp = lax.axis_index("fs"), lax.axis_index("tp")
    spread = fs_count // experts
    mine, half = me // spread, lax.rem(me, spread)
    group = spread * tp_count
    index = half * tp_count + my_tp
    barrier = pltpu.get_barrier_semaphore()

    def mate(s):
        other = lax.rem(index + s, group)
        return other, other // tp_count, lax.rem(other, tp_count)

    def partner(s):
        return lax.rem(mine + s, experts)

    for s in range(1, group):
        _, h, t = mate(s)
        pl.semaphore_signal(
            barrier, inc=1, device_id={"fs": mine * spread + h, "tp": t}, device_id_type=MESH
        )
    for s in range(1, experts):
        pl.semaphore_signal(
            barrier, inc=1, device_id={"fs": partner(s) * spread + half}, device_id_type=MESH
        )
    pl.semaphore_wait(barrier, group + experts - 2)

    def copy1(s):
        _, h, t = mate(s)
        return pltpu.make_async_remote_copy(
            src_ref=part_ref.at[h, t], dst_ref=first.at[s], send_sem=send1.at[s],
            recv_sem=recv1.at[s], device_id={"fs": mine * spread + h, "tp": t},
            device_id_type=MESH,
        )

    for s in range(1, group):
        copy1(s).start()
    keep = pltpu.make_async_copy(part_ref.at[half, my_tp], first.at[0], keep_sem)
    keep.start()
    keep.wait()
    acc = first[0].astype(jnp.float32)
    for s in range(1, group):
        copy1(s).wait_recv()
        acc = acc + first[s].astype(jnp.float32)
    total[...] = acc.astype(jnp.bfloat16)

    def copy2(s):
        return pltpu.make_async_remote_copy(
            src_ref=total.at[partner(s)], dst_ref=second.at[s], send_sem=send2.at[s],
            recv_sem=recv2.at[s], device_id={"fs": partner(s) * spread + half},
            device_id_type=MESH,
        )

    for s in range(1, experts):
        copy2(s).start()
    result = total[mine].astype(jnp.float32)
    for s in range(1, experts):
        copy2(s).wait_recv()
        result = result + second[s].astype(jnp.float32)
    out_ref[...] = result.astype(jnp.bfloat16)
    for s in range(1, group):
        copy1(s).wait_send()
    for s in range(1, experts):
        copy2(s).wait_send()


def reduce(part, fs_count, tp_count):
    spread, _, experts, own, columns = part.shape
    group = spread * tp_count
    bf16, dma = jnp.bfloat16, pltpu.SemaphoreType.DMA
    return pl.pallas_call(
        functools.partial(reduce_kernel, fs_count, tp_count, experts),
        in_specs=[pl.BlockSpec(memory_space=pltpu.VMEM)],
        out_specs=pl.BlockSpec(memory_space=pltpu.VMEM),
        out_shape=jax.ShapeDtypeStruct((own, columns), bf16),
        scratch_shapes=[
            pltpu.VMEM((group, experts, own, columns), bf16),
            pltpu.VMEM((experts, own, columns), bf16),
            pltpu.VMEM((experts, own, columns), bf16),
            dma((group,)), dma((group,)), dma((experts,)), dma((experts,)), dma,
        ],
        compiler_params=pltpu.CompilerParams(
            collective_id=1, has_side_effects=True, vmem_limit_bytes=48 * 1024 * 1024
        ),
    )(part)


def gate_kernel(x_ref, w_ref, act_ref, copy_ref):
    copy_ref[...] = w_ref[...]
    part = jnp.dot(x_ref[0], w_ref[0], preferred_element_type=jnp.float32)

    @pl.when(pl.program_id(0) == 0)
    def _():
        act_ref[...] = part

    @pl.when(pl.program_id(0) > 0)
    def _():
        act_ref[...] += part


def up_kernel(x_ref, w_ref, gate_ref, hidden_ref, copy_ref, acc_ref):
    copy_ref[...] = w_ref[...]
    part = jnp.dot(x_ref[0], w_ref[0], preferred_element_type=jnp.float32)

    @pl.when(pl.program_id(0) == 0)
    def _():
        acc_ref[...] = part

    @pl.when(pl.program_id(0) > 0)
    def _():
        acc_ref[...] += part

    @pl.when(pl.program_id(0) == pl.num_programs(0) - 1)
    def _():
        gate = gate_ref[...]
        hidden_ref[...] = (gate / (1.0 + jnp.exp(-gate)) * acc_ref[...]).astype(jnp.bfloat16)


def project(rows, local, gate_act=None):
    count, width, block = local.shape
    tokens = rows.shape[1]
    per_tp = count // rows.shape[0]
    in_specs = [
        pl.BlockSpec((1, tokens, width), lambda g: (g // per_tp, 0, g % per_tp)),
        pl.BlockSpec((1, width, block), lambda g: (g, 0, 0)),
    ]
    operands = [rows, local]
    scratch = []
    kernel, act_type = gate_kernel, jnp.float32
    if gate_act is not None:
        in_specs.append(pl.BlockSpec((tokens, block), lambda g: (0, 0)))
        operands.append(gate_act)
        scratch = [pltpu.VMEM((tokens, block), jnp.float32)]
        kernel, act_type = up_kernel, jnp.bfloat16
    return pl.pallas_call(
        kernel,
        grid=(count,),
        in_specs=in_specs,
        out_specs=[
            pl.BlockSpec((tokens, block), lambda g: (0, 0)),
            pl.BlockSpec((1, width, block), lambda g: (0, g, 0)),
        ],
        out_shape=[
            jax.ShapeDtypeStruct((tokens, block), act_type),
            jax.ShapeDtypeStruct((1, count * width, block), jnp.bfloat16),
        ],
        scratch_shapes=scratch,
        compiler_params=pltpu.CompilerParams(vmem_limit_bytes=VMEM_LIMIT),
        cost_estimate=pl.CostEstimate(
            flops=2 * tokens * count * width * block,
            bytes_accessed=count * width * block * 4,
            transcendentals=0,
        ),
    )(*operands)


def down_kernel(hidden_ref, weight_ref, w_ref, *rest):
    part_ref, copy_ref = rest[-2:]
    copy_ref[...] = w_ref[...]
    part = lax.dot_general(
        hidden_ref[...], w_ref[0], (((1,), (1,)), ((), ())), preferred_element_type=jnp.float32
    )
    part = part * weight_ref[...]
    spread, _, experts, own, width = part_ref.shape
    blocks = part.reshape(experts, spread, own, width).astype(part_ref.dtype)
    for h in range(spread):
        part_ref[h, 0] = blocks[:, h]


def project_back(hidden, weight, local, so_far, piece, pieces, experts, spread, tp_count):
    count, width, block = local.shape
    tokens = hidden.shape[0]
    per_tp = count // tp_count
    own = tokens // count
    in_specs = [
        pl.BlockSpec((tokens, block), lambda g: (0, 0)),
        pl.BlockSpec((tokens, 1), lambda g: (0, 0)),
        pl.BlockSpec((1, width, block), lambda g: (g, 0, 0)),
    ]
    operands = [hidden, weight, local]
    aliases = {}
    if so_far is not None:
        in_specs.append(pl.BlockSpec(memory_space=pl.ANY))
        operands.append(so_far)
        aliases = {3: 1}
    return pl.pallas_call(
        down_kernel,
        grid=(count,),
        in_specs=in_specs,
        out_specs=[
            pl.BlockSpec(
                (spread, 1, experts, own, width),
                lambda g: (0, g // per_tp, 0, 0, g % per_tp),
            ),
            pl.BlockSpec((1, width, block), lambda g: (0, g * pieces + piece, 0)),
        ],
        out_shape=[
            jax.ShapeDtypeStruct(
                (spread, tp_count, experts, own, per_tp * width), jnp.bfloat16
            ),
            jax.ShapeDtypeStruct((1, count * width * pieces, block), jnp.bfloat16),
        ],
        input_output_aliases=aliases,
        compiler_params=pltpu.CompilerParams(vmem_limit_bytes=VMEM_LIMIT),
        cost_estimate=pl.CostEstimate(
            flops=2 * tokens * count * width * block,
            bytes_accessed=count * width * block * 4 + tokens * count * width * 4,
            transcendentals=0,
        ),
    )(*operands)


def swap(pieces):
    return lax.all_to_all(pieces, "fs", split_axis=0, concat_axis=0, tiled=True)


def per_device(tokens, routes, route_logits, norm_gain, gate_weight, up_weight, down_weight):
    experts, width, _ = gate_weight.shape
    fs_count, tp_count = lax.axis_size("fs"), lax.axis_size("tp")
    spread = fs_count // experts
    own, model = tokens.shape
    part_width = model // tp_count
    pieces = 2 if width % 256 == 0 else 1
    rows, weights, gate_local, up_local, down_local, rest = exchange(
        tokens, routes, route_logits, norm_gain[:, None],
        gate_weight, up_weight, down_weight, fs_count, tp_count, pieces,
    )
    rows = rows.reshape(tp_count, fs_count * own, part_width)
    mine = lax.axis_index("fs") // spread
    weight = lax.dynamic_slice_in_dim(weights.reshape(fs_count * own, -1), mine, 1, 1)
    locals_ = [down_local]
    if pieces > 1:
        locals_.append(swap(rest))
    gate_act, gate_out = project(rows, gate_local)
    hidden, up_out = project(rows, up_local, gate_act)
    down_out, sums = None, []
    for p in range(pieces):
        part, down_out = project_back(
            hidden, weight, locals_[p], down_out, p, pieces, experts, spread, tp_count
        )
        summed = reduce(part, fs_count, tp_count)
        sums.append(summed.reshape(own, part_width // width, 1, width // pieces))
    mixed = jnp.concatenate(sums, axis=2).reshape(own, part_width)
    return (mixed, gate_out, up_out, down_out)


def solution(mesh):
    in_specs = (
        P("fs", None),
        P("fs", None),
        P("fs", None),
        P("fs"),
        P(None, "fs", "tp"),
        P(None, "fs", "tp"),
        P(None, "fs", "tp"),
    )
    out_specs = (P("fs", "tp"), P("tp", None, "fs"), P("tp", None, "fs"), P("tp", None, "fs"))
    return jax.shard_map(
        per_device, mesh=mesh, in_specs=in_specs, out_specs=out_specs, check_vma=False
    )
```

profile of v0, /device:TPU:0, one launch (start us, length us, event | category | flops | bytes accessed | tf_op | source)
XLA Modules:
  0.0 611.0 jit_solution(3214226057202407041)
XLA Ops:
  0.6 1.4 copy.15.routes_ref
  2.0 1.4 copy.16.logits_ref
  3.4 1.5 copy.17.gain_ref
  4.9 476.8 %shard_map.102 = (bf16[4,8,40,1024]{3,2,1,0:T(8,128)(2,1)}, f32[8,40,128]{2,1,0:T(8,128)}, bf16[8,512,1024]{2,1,0:T(8,128)(2,1)}, bf16[8,512,1024]{2,1,0:T(8,128...) custom-call(bf16[40,4096]{1,0:T(8,128)(2,1)} %tok_ref.1, s32[40,2]{1,0:T(8,128)} %copy.15.routes_ref, ...), custom_call_target="tpu_custom_call" | custom-call | tf_op jit(solution)/shard_map/pallas_call | solution.py:187
  481.8 0.0 copy-start.4
  481.8 0.0 copy-start
  481.8 4.8 all-to-all-start
  486.6 0.0 copy-done.4
  486.6 0.1 constant_dynamic-slice_fusion.weight_ref
  486.7 0.0 copy-done
  486.8 0.0 copy-start.2
  486.8 3.4 copy-done.2
  490.1 0.0 copy-start.3
  490.1 7.5 %shard_map.103 = (f32[320,1024]{1,0:T(8,128)S(1)}, bf16[1,4096,1024]{2,1,0:T(8,128)(2,1)}) custom-call(bf16[4,320,1024]{2,1,0:T(8,128)(2,1)S(1)} %bitcast.3, bf16[8,512,1024]{2,1,0:T(8,128)(2,1)S(1)} %copy-done.2), custom_call_target="tpu_custom_call" | custom-call | flops 2684354560 | bytes 16777216 | tf_op jit(solution)/shard_map/pallas_call | solution.py:353
  497.6 0.0 copy-start.1
  497.6 3.4 copy-done.1
  501.0 7.8 %shard_map.104 = (bf16[320,1024]{1,0:T(8,128)(2,1)S(1)}, bf16[1,4096,1024]{2,1,0:T(8,128)(2,1)}) custom-call(bf16[4,320,1024]{2,1,0:T(8,128)(2,1)S(1)} %bitcast.4, bf16[8,512,1024]{2,1,0:T(8,128)(2,1)S(1)} %copy-done.1, f32[320,1024]{1,0:T(8,128)S(1)} %get-tuple-element.21.gate_ref), custom_call_target="tpu_custom_call" | custom-call | flops 2684354560 | bytes 16777216 | tf_op jit(solution)/shard_map/pallas_call | solution.py:353
  508.8 0.0 copy-done.3
  508.8 5.2 shard_map.105
  514.0 68.9 %shard_map.106 = bf16[40,512]{1,0:T(8,128)(2,1)S(1)} custom-call(bf16[2,4,4,40,512]{4,3,2,1,0:T(8,128)(2,1)S(1)} %get-tuple-element.25.part_ref), custom_call_target="tpu_custom_call" | custom-call | tf_op jit(solution)/shard_map/pallas_call | solution.py:289
  583.0 0.0 all-to-all-done.w_ref
  583.0 7.9 %shard_map.107 = (bf16[2,4,4,40,512]{4,3,2,1,0:T(8,128)(2,1)S(1)}, bf16[1,4096,1024]{2,1,0:T(8,128)(2,1)}) custom-call(bf16[320,1024]{1,0:T(8,128)(2,1)S(1)} %get-tuple-element.22.hidden_ref, f32[320,1]{1,0:T(8,128)S(1)} %constant_dynamic-slice_fusion.weight_ref, bf16[8,256,1024]{2,1,0:T(8,128)(2,1)} %all-to-all-done.w_ref, ...), custom_call_target="tpu_custom_call", output_to_operand_aliasing={{1}: (3, {})} | custom-call | flops 1342177280 | bytes 11010048 | tf_op jit(solution)/shard_map/pallas_call | solution.py:404
  590.9 19.2 %shard_map.108 = bf16[40,512]{1,0:T(8,128)(2,1)S(1)} custom-call(bf16[2,4,4,40,512]{4,3,2,1,0:T(8,128)(2,1)S(1)} %get-tuple-element.28.part_ref), custom_call_target="tpu_custom_call" | custom-call | tf_op jit(solution)/shard_map/pallas_call | solution.py:289
  610.1 0.1 pad_maximum_fusion
  610.3 0.1 copy.18
  610.3 0.7 reshape.27
  (2 shorter events, 0.0 us)
Async XLA Ops:
  481.8 4.9 copy-start.4
  481.8 5.0 copy-start
  481.8 101.2 %all-to-all-start = ((bf16[8,256,1024]{2,1,0:T(8,128)(2,1)}), bf16[8,256,1024]{2,1,0:T(8,128)(2,1)}, u32[]{:S(2)}, u32[]{:S(2)}) async-start(bf16[8,256,1024]{2,1,0:T(8,128)(2,1)} %get-tuple-element.26), calls=%async_computation | async-start | bytes 8388608 | tf_op jit(solution)/shard_map/all_to_all | solution.py:432
  486.8 3.4 copy-start.2
  490.1 18.7 %copy-start.3 = (bf16[8,256,1024]{2,1,0:T(8,128)(2,1)S(1)}, bf16[8,256,1024]{2,1,0:T(8,128)(2,1)}, u32[]{:S(2)}) copy-start(bf16[8,256,1024]{2,1,0:T(8,128)(2,1)} %get-tuple-element.24.w_ref) | copy-start | bytes 12582916
  497.6 3.4 copy-start.1
where the time goes:
time: 613 us; the launch traced here: 611 us
  Pallas kernels  593 us (97%)
  local copies, waits for them, and re-layouts  11.9 us (2%)
    pallas_call x1, Pallas kernels, exchange(): pl.pallas_call(functools.partial(exchange_kernel, fs_count, tp_count, exp...  477 us
    pallas_call x2, Pallas kernels, reduce(): pl.pallas_call(functools.partial(reduce_kernel, fs_count, tp_count, exper...  88.1 us
    pallas_call x2, Pallas kernels, project(): pl.pallas_call(kernel, grid=(count,), in_specs=in_specs, out_specs=[pl.Bl...  15.3 us
    pallas_call x2, Pallas kernels, project_back(): pl.pallas_call(down_kernel, grid=(count,), in_specs=in_specs, out_specs=[...  13.1 us
  transfers between devices with their start and end apart: 1, of which 0 were waited for; matrix products, arithmetic and copies ran while one was open for 0% of the time, Pallas kernels for 15%

commit v1 on v0

v1 whole, which is shorter than its diff:
```python
import functools

import jax
import jax.numpy as jnp
from jax import lax
from jax.experimental import pallas as pl
from jax.experimental.pallas import tpu as pltpu
from jax.sharding import PartitionSpec as P

MESH = pl.DeviceIdType.MESH
F32, BF16 = jnp.float32, jnp.bfloat16


def wait_bytes(ref, sem):
    pltpu.make_async_copy(ref, ref, sem).wait()


def loop(count, body):
    def step(i, carry):
        body(i)
        return carry

    lax.fori_loop(0, count, step, 0)


def fused_kernel(
    fs_count, tp_count, experts, pieces,
    tok_ref, routes_ref, logits_ref, gain_ref, gate_hbm, up_hbm, down_hbm,
    mixed_out, gate_out, up_out, down_out,
    stage, gate_send, up_send, down_send, down_recv, wbuf,
    xown, xcol, x_all, act, hidden, part, rs_recv, total, home,
    load_sem, send_sem, recv_sem, keep_sem, down_sem, down_keep, x_sem, wload_sem,
    rs_send_sem, rs_recv_sem, home_send, home_recv,
):
    me, my_tp = lax.axis_index("fs"), lax.axis_index("tp")
    spread = fs_count // experts
    mine, inner = me // spread, lax.rem(me, spread)
    group = spread * tp_count
    index = inner * tp_count + my_tp
    half = fs_count // 2
    side = me // half
    share = fs_count // tp_count
    own, model = tok_ref.shape
    width, block = stage.shape[1], stage.shape[2]
    rows = width // pieces
    tokens = fs_count * own
    pairs = tp_count // 2
    rounds = 2 * pieces
    owner_fs, owner_tp = me // tp_count, lax.rem(me, tp_count)

    def send_order(step):
        far = (1 - side) * half + lax.rem(me + step, half)
        near = side * half + lax.rem(me + 1 + step, half)
        return jnp.where(step < half, far, near)

    def near_source(k):
        return side * half + lax.rem(me + 2 * half - 1 - k, half)

    def far_source(k):
        return (1 - side) * half + lax.rem(me + half - k, half)

    def gather_peer(s):
        other = lax.rem(my_tp * share + lax.rem(inner, share) + s, fs_count)
        fs = mine * spread + (inner // share) * share + lax.rem(other, share)
        return fs, other // share

    def plane_peer(i):
        return mine * spread + i // tp_count, lax.rem(i, tp_count)

    barrier = pltpu.get_barrier_semaphore()

    def signal(fs, tp):
        pl.semaphore_signal(
            barrier, inc=1, device_id={"fs": fs, "tp": tp}, device_id_type=MESH
        )

    def load(hbm, step, slot):
        dst = send_order(step)
        column = pl.multiple_of(lax.rem(dst, spread) * block, block)
        return pltpu.make_async_copy(
            hbm.at[dst // spread, :, pl.ds(column, block)], stage.at[slot], load_sem.at[slot]
        )

    load(gate_hbm, 0, 0).start()
    loop(fs_count - 1, lambda s: signal(lax.rem(me + 1 + s, fs_count), my_tp))

    def greet(s):
        fs, tp = plane_peer(lax.rem(index + 1 + s, group))
        signal(fs, tp)

    loop(group - 1, greet)

    def sender_of(e):
        return e * spread + owner_fs, owner_tp

    def is_self(fs, tp):
        return jnp.logical_and(fs == me, tp == my_tp)

    for e in range(experts):
        fs, tp = sender_of(e)

        @pl.when(jnp.logical_not(is_self(fs, tp)))
        def _(fs=fs, tp=tp):
            signal(fs, tp)

    tok = tok_ref[...].astype(F32)
    scale = lax.rsqrt(jnp.mean(tok * tok, axis=1, keepdims=True) + 1e-05)
    for j in range(share):
        column = pl.multiple_of((my_tp * share + j) * width, width)
        cols = tok_ref[:, pl.ds(column, width)].astype(F32)
        xown[j] = (cols * scale).astype(BF16)
    xcol[me] = xown[lax.rem(inner, share)]

    homes = jnp.where(index < fs_count, tp_count, 0) - jnp.where(index == me, 1, 0)
    pl.semaphore_wait(barrier, fs_count + group - 2 + homes)

    def x_send(s):
        dst = send_order(s)
        pltpu.make_async_remote_copy(
            src_ref=xown.at[lax.rem(lax.rem(dst, spread), share)], dst_ref=xcol.at[me],
            send_sem=x_sem.at[0], recv_sem=x_sem.at[1], device_id={"fs": dst},
            device_id_type=MESH,
        ).start()

    loop(fs_count - 1, x_send)

    def block_copy(m, held, out, dst):
        return pltpu.make_async_remote_copy(
            src_ref=held.at[dst], dst_ref=out.at[me], send_sem=send_sem.at[m],
            recv_sem=recv_sem.at[m, me], device_id={"fs": dst}, device_id_type=MESH,
        )

    def piece_copy(p, dst):
        span = pl.ds(pl.multiple_of(p * rows, rows), rows)
        return pltpu.make_async_remote_copy(
            src_ref=down_send.at[dst, span], dst_ref=down_recv.at[me, span],
            send_sem=send_sem.at[2], recv_sem=down_sem.at[p, me], device_id={"fs": dst},
            device_id_type=MESH,
        )

    def convert(m, hbm, following):
        def body(step):
            slot = lax.rem(m * fs_count + step, 2)
            dst = send_order(step)

            @pl.when(step + 1 < fs_count)
            def _():
                load(hbm, step + 1, 1 - slot).start()

            if following is not None:

                @pl.when(step + 1 == fs_count)
                def _():
                    load(following, 0, 1 - slot).start()

            load(hbm, step, slot).wait()
            if m < 2:
                held, out = ((gate_send, gate_out), (up_send, up_out))[m]
                held[dst] = (stage[slot] * gain_ref[...]).astype(BF16)

                @pl.when(dst == me)
                def _():
                    pltpu.make_async_copy(held.at[me], out.at[me], keep_sem.at[m]).start()

                @pl.when(dst != me)
                def _():
                    block_copy(m, held, out, dst).start()
            else:

                @pl.when(dst == me)
                def _():
                    down_recv[me] = stage[slot].astype(BF16)

                @pl.when(dst != me)
                def _():
                    down_send[dst] = stage[slot].astype(BF16)

        loop(fs_count, body)

    convert(0, gate_hbm, up_hbm)

    wait_bytes(xcol.at[pl.ds(0, fs_count - 1)], x_sem.at[1])
    held_part = my_tp * share + lax.rem(inner, share)

    def x_gather(s):
        fs, tp = gather_peer(s + 1)
        pltpu.make_async_remote_copy(
            src_ref=xcol, dst_ref=x_all.at[held_part], send_sem=x_sem.at[2],
            recv_sem=x_sem.at[3], device_id={"fs": fs, "tp": tp}, device_id_type=MESH,
        ).start()

    loop(fs_count - 1, x_gather)
    x_all[held_part] = xcol[...]

    convert(1, up_hbm, down_hbm)
    convert(2, down_hbm, None)
    loop(pieces, lambda p: loop(fs_count - 1, lambda s: piece_copy(p, send_order(s)).start()))

    wait_bytes(x_all.at[pl.ds(0, fs_count - 1)], x_sem.at[3])

    def project(m, held, out, a):
        act[a] = jnp.zeros_like(act[a])

        def body(k):
            g = jnp.where(k < half, near_source(k), far_source(k - half))

            @pl.when(g == me)
            def _():
                wait_bytes(held.at[me], keep_sem.at[m])

            @pl.when(g != me)
            def _():
                wait_bytes(out.at[g], recv_sem.at[m, g])

            fetch = pltpu.make_async_copy(out.at[g], wbuf, wload_sem)
            fetch.start()
            x = x_all[g].astype(F32).reshape(tokens, width).astype(BF16)
            fetch.wait()
            act[a] += jnp.dot(x, wbuf[...], preferred_element_type=F32)

        loop(fs_count, body)

    project(0, gate_send, gate_out, 0)
    project(1, up_send, up_out, 1)
    gate = act[0]
    hidden[...] = (gate / (1.0 + jnp.exp(-gate)) * act[1]).astype(BF16)

    def base_of(r):
        return jnp.where(lax.rem(r, 2) == 0, side, 1 - side) * half

    def finish(r):
        p = r // 2
        wait_bytes(rs_recv.at[r], rs_recv_sem.at[r])

        def add(s, acc):
            return acc + rs_recv[r, s].astype(F32)

        acc = lax.fori_loop(0, group - 1, add, part[r, index].astype(F32))
        total[r] = acc.astype(BF16)
        for q in range(pairs):
            tp = base_of(r) // share + q

            @pl.when(is_self(index, tp))
            def _(q=q):
                home[mine, p] = total[r, pl.ds(q * share, share)]

            @pl.when(jnp.logical_not(is_self(index, tp)))
            def _(q=q, tp=tp):
                home_copy(r, q, tp).start()

    def home_copy(r, q, tp):
        return pltpu.make_async_remote_copy(
            src_ref=total.at[r, pl.ds(q * share, share)], dst_ref=home.at[mine, r // 2],
            send_sem=home_send.at[r, q], recv_sem=home_recv.at[r // 2, mine],
            device_id={"fs": index, "tp": tp}, device_id_type=MESH,
        )

    def run_round(r):
        p = r // 2
        span = pl.ds(pl.multiple_of(p * rows, rows), rows)

        def item(k):
            g = jnp.where(lax.rem(r, 2) == 0, near_source(k), far_source(k))

            @pl.when(g != me)
            def _():
                wait_bytes(down_recv.at[g, span], down_sem.at[p, g])

            pltpu.make_async_copy(
                down_recv.at[g, span], down_out.at[g, span], down_keep
            ).start()
            out = lax.dot_general(
                hidden[...], down_recv[g, span], (((1,), (1,)), ((), ())),
                preferred_element_type=F32,
            )
            part[r, :, g - base_of(r)] = out.reshape(fs_count, own, rows).astype(BF16)

        loop(half, item)

        def rs_send(s):
            i = lax.rem(index + 1 + s, fs_count)

            @pl.when(i != index)
            def _():
                fs, tp = plane_peer(i)
                slot = lax.rem(index + 2 * group - i - 1, group)
                pltpu.make_async_remote_copy(
                    src_ref=part.at[r, i], dst_ref=rs_recv.at[r, slot],
                    send_sem=rs_send_sem.at[r], recv_sem=rs_recv_sem.at[r],
                    device_id={"fs": fs, "tp": tp}, device_id_type=MESH,
                ).start()

        loop(fs_count, rs_send)

        @pl.when(jnp.logical_and(r > 0, index < fs_count))
        def _():
            finish(r - 1)

    loop(rounds, run_round)

    @pl.when(index < fs_count)
    def _():
        finish(rounds - 1)

    first, second = logits_ref[:, 0:1], logits_ref[:, 1:2]
    share_first = 1.0 / (1.0 + jnp.exp(second - first))
    share_second = 1.0 / (1.0 + jnp.exp(first - second))
    for p in range(pieces):
        mixed = [jnp.zeros((own, rows), F32)] * share
        for e in range(experts):

            @pl.when(jnp.logical_not(is_self(*sender_of(e))))
            def _(e=e, p=p):
                wait_bytes(home.at[e, p], home_recv.at[p, e])

            weight = jnp.where(routes_ref[:, 0:1] == e, share_first, 0.0) + jnp.where(
                routes_ref[:, 1:2] == e, share_second, 0.0
            )
            for j in range(share):
                mixed[j] = mixed[j] + weight * home[e, p, j].astype(F32)
        for j in range(share):
            column = j * width + p * rows
            mixed_out[:, column : column + rows] = mixed[j].astype(BF16)

    wait_bytes(down_recv, down_keep)
    wait_bytes(xcol.at[pl.ds(0, fs_count - 1)], x_sem.at[0])
    wait_bytes(x_all.at[pl.ds(0, fs_count - 1)], x_sem.at[2])
    for m, held in enumerate((gate_send, up_send, down_send)):
        wait_bytes(held.at[pl.ds(0, fs_count - 1)], send_sem.at[m])

    def drain(r):
        @pl.when(index < fs_count)
        def _():
            wait_bytes(part.at[r, pl.ds(0, fs_count - 1)], rs_send_sem.at[r])
            for q in range(pairs):
                tp = base_of(r) // share + q

                @pl.when(jnp.logical_not(is_self(index, tp)))
                def _(q=q):
                    wait_bytes(total.at[r, pl.ds(q * share, share)], home_send.at[r, q])

        @pl.when(index >= fs_count)
        def _():
            wait_bytes(part.at[r], rs_send_sem.at[r])

    loop(rounds, drain)


def per_device(tokens, routes, route_logits, norm_gain, gate_weight, up_weight, down_weight):
    experts, width, columns = gate_weight.shape
    fs_count, tp_count = lax.axis_size("fs"), lax.axis_size("tp")
    spread = fs_count // experts
    block = columns // spread
    own, model = tokens.shape
    group = spread * tp_count
    half, share = fs_count // 2, fs_count // tp_count
    pieces = max(1, width // 128)
    rows = width // pieces
    rounds = 2 * pieces
    dma = pltpu.SemaphoreType.DMA
    vmem = pl.BlockSpec(memory_space=pltpu.VMEM)
    anywhere = pl.BlockSpec(memory_space=pl.ANY)
    landed = jax.ShapeDtypeStruct((fs_count, width, block), BF16)
    mixed, *landings = pl.pallas_call(
        functools.partial(fused_kernel, fs_count, tp_count, experts, pieces),
        in_specs=[vmem] * 4 + [anywhere] * 3,
        out_specs=[vmem] + [anywhere] * 3,
        out_shape=[jax.ShapeDtypeStruct((own, model // tp_count), BF16)] + [landed] * 3,
        scratch_shapes=[
            pltpu.VMEM((2, width, block), F32),
            pltpu.VMEM((fs_count, width, block), BF16),
            pltpu.VMEM((fs_count, width, block), BF16),
            pltpu.VMEM((fs_count, width, block), BF16),
            pltpu.VMEM((fs_count, width, block), BF16),
            pltpu.VMEM((width, block), BF16),
            pltpu.VMEM((share, own, width), BF16),
            pltpu.VMEM((fs_count, own, width), BF16),
            pltpu.VMEM((fs_count, fs_count, own, width), BF16),
            pltpu.VMEM((2, fs_count * own, block), F32),
            pltpu.VMEM((fs_count * own, block), BF16),
            pltpu.VMEM((rounds, fs_count, half, own, rows), BF16),
            pltpu.VMEM((rounds, group - 1, half, own, rows), BF16),
            pltpu.VMEM((rounds, half, own, rows), BF16),
            pltpu.VMEM((experts, pieces, share, own, rows), BF16),
            dma((2,)), dma((3,)), dma((2, fs_count)), dma((2,)), dma((pieces, fs_count)), dma,
            dma((4,)), dma, dma((rounds,)), dma((rounds,)), dma((rounds, tp_count // 2)),
            dma((pieces, experts)),
        ],
        compiler_params=pltpu.CompilerParams(
            collective_id=0, has_side_effects=True, vmem_limit_bytes=63 * 1024 * 1024
        ),
    )(
        tokens, routes, route_logits, norm_gain[:, None], gate_weight, up_weight, down_weight
    )
    return (mixed, *(x.reshape(1, fs_count * width, block) for x in landings))


def solution(mesh):
    in_specs = (
        P("fs", None),
        P("fs", None),
        P("fs", None),
        P("fs"),
        P(None, "fs", "tp"),
        P(None, "fs", "tp"),
        P(None, "fs", "tp"),
    )
    out_specs = (P("fs", "tp"), P("tp", None, "fs"), P("tp", None, "fs"), P("tp", None, "fs"))
    return jax.shard_map(
        per_device, mesh=mesh, in_specs=in_specs, out_specs=out_specs, check_vma=False
    )
```

time: 613 us -> 622 us (1.015)
  local copies, waits for them, and re-layouts: 11.9 us -> 29.1 us
    unnamed x12 -> x6, local copies, waits for them, and re-layouts: 9.5 us -> 27.5 us
    pallas_call x7 -> x1, Pallas kernels: 593 us -> 591 us  [per_device(): pl.pallas_call(functools.partial(fused_kernel, fs_count, tp_count, expert...]
  transfers between devices with their start and end apart: 1 -> 0, of which waited for: 0 -> 0; matrix products, arithmetic and copies ran while one was open for 0% -> 0% of each run, Pallas kernels for 15% -> 0%
where the time goes in v1:
time: 622 us; the launch traced here: 621 us
  Pallas kernels  591 us (95%)
  local copies, waits for them, and re-layouts  29.1 us (5%)
    pallas_call x1, Pallas kernels, per_device(): pl.pallas_call(functools.partial(fused_kernel, fs_count, tp_count, expert...  591 us
    unnamed x6, local copies, waits for them, and re-layouts  27.5 us

profile of v1, /device:TPU:0, one launch (start us, length us, event | category | flops | bytes accessed | tf_op | source)
XLA Modules:
  0.0 620.9 jit_solution(6092590893611037890)
XLA Ops:
  0.6 1.4 copy.13.routes_ref
  2.0 1.4 copy.14.logits_ref
  3.4 1.5 copy.15.gain_ref
  4.9 591.2 %shard_map.102 = (bf16[40,1024]{1,0:T(8,128)(2,1)}, bf16[8,512,1024]{2,1,0:T(8,128)(2,1)}, bf16[8,512,1024]{2,1,0:T(8,128)(2,1)}, bf16[8,512,1024]{2,1,0:T(8,128)(2,1)}) custom-call(bf16[40,4096]{1,0:T(8,128)(2,1)} %tok_ref.1, s32[40,2]{1,0:T(8,128)} %copy.13.routes_ref, f32[40,2]{1,0:T(8,128)} %copy.14.logits_ref, f32[512,1]{1,0:T(8,128)} %copy.15.gain_ref, ...), custom_call_target="tpu_custom_call" | custom-call | tf_op jit(solution)/shard_map/pallas_call | solution.py:364
  596.1 1.5 copy.20
  597.7 7.8 %copy.21 = bf16[1,4096,1024]{2,1,0:T(8,128)(2,1)} copy(bf16[1,4096,1024]{2,1,0:T(8,128)(2,1)} %bitcast.6) | data formatting | bytes 16777216
  605.4 7.8 %copy.22 = bf16[1,4096,1024]{2,1,0:T(8,128)(2,1)} copy(bf16[1,4096,1024]{2,1,0:T(8,128)(2,1)} %bitcast.5) | data formatting | bytes 16777216
  613.2 7.8 %copy.23 = bf16[1,4096,1024]{2,1,0:T(8,128)(2,1)} copy(bf16[1,4096,1024]{2,1,0:T(8,128)(2,1)} %bitcast.4) | data formatting | bytes 16777216

commit v2 on v1

--- a/solution.py
+++ b/solution.py
@@ -9,6 +9,7 @@
 
 MESH = pl.DeviceIdType.MESH
 F32, BF16 = jnp.float32, jnp.bfloat16
+VMEM_BYTES = 60 * 1024 * 1024
 
 
 def wait_bytes(ref, sem):
@@ -23,13 +24,24 @@
     lax.fori_loop(0, count, step, 0)
 
 
+def store_kernel(*refs):
+    count = (len(refs) - 1) // 2
+    held, out, sem = refs[:count], refs[count : 2 * count], refs[-1]
+    pltpu.make_async_copy(held[0], out[0], sem.at[0]).start()
+    for i in range(1, count):
+        for g in range(held[i].shape[0]):
+            pltpu.make_async_copy(held[i].at[g], out[i].at[g], sem.at[i]).start()
+    for i in range(count):
+        pltpu.make_async_copy(held[i], out[i], sem.at[i]).wait()
+
+
 def fused_kernel(
     fs_count, tp_count, experts, pieces,
     tok_ref, routes_ref, logits_ref, gain_ref, gate_hbm, up_hbm, down_hbm,
-    mixed_out, gate_out, up_out, down_out,
-    stage, gate_send, up_send, down_send, down_recv, wbuf,
+    mixed_out, gate_out, up_out, down_out, up_send, down_send,
+    stage, gate_send, packed, turn, gain_col,
     xown, xcol, x_all, act, hidden, part, rs_recv, total, home,
-    load_sem, send_sem, recv_sem, keep_sem, down_sem, down_keep, x_sem, wload_sem,
+    load_sem, store_sem, send_sem, recv_sem, down_sem, x_sem,
     rs_send_sem, rs_recv_sem, home_send, home_recv,
 ):
     me, my_tp = lax.axis_index("fs"), lax.axis_index("tp")
@@ -49,9 +61,7 @@
     owner_fs, owner_tp = me // tp_count, lax.rem(me, tp_count)
 
     def send_order(step):
-        far = (1 - side) * half + lax.rem(me + step, half)
-        near = side * half + lax.rem(me + 1 + step, half)
-        return jnp.where(step < half, far, near)
+        return lax.rem(me + half + step, fs_count)
 
     def near_source(k):
         return side * half + lax.rem(me + 2 * half - 1 - k, half)
@@ -102,6 +112,12 @@
         @pl.when(jnp.logical_not(is_self(fs, tp)))
         def _(fs=fs, tp=tp):
             signal(fs, tp)
+
+    turn[...] = jnp.zeros_like(turn)
+    turn[: gain_ref.shape[0]] = gain_ref[...]
+    turned = turn[...].T
+    for q in range(width // 128):
+        gain_col[q * 128 : (q + 1) * 128] = turned[:, q : q + 1]
 
     tok = tok_ref[...].astype(F32)
     scale = lax.rsqrt(jnp.mean(tok * tok, axis=1, keepdims=True) + 1e-05)
@@ -115,7 +131,7 @@
     pl.semaphore_wait(barrier, fs_count + group - 2 + homes)
 
     def x_send(s):
-        dst = send_order(s)
+        dst = lax.rem(me + 1 + s, fs_count)
         pltpu.make_async_remote_copy(
             src_ref=xown.at[lax.rem(lax.rem(dst, spread), share)], dst_ref=xcol.at[me],
             send_sem=x_sem.at[0], recv_sem=x_sem.at[1], device_id={"fs": dst},
@@ -133,7 +149,7 @@
     def piece_copy(p, dst):
         span = pl.ds(pl.multiple_of(p * rows, rows), rows)
         return pltpu.make_async_remote_copy(
-            src_ref=down_send.at[dst, span], dst_ref=down_recv.at[me, span],
+            src_ref=down_send.at[dst, span], dst_ref=down_out.at[me, span],
             send_sem=send_sem.at[2], recv_sem=down_sem.at[p, me], device_id={"fs": dst},
             device_id_type=MESH,
         )
@@ -154,28 +170,49 @@
                     load(following, 0, 1 - slot).start()
 
             load(hbm, step, slot).wait()
+            held, out = ((gate_send, gate_out), (up_send, up_out), (down_send, down_out))[m]
+            block_f32 = stage[slot]
             if m < 2:
-                held, out = ((gate_send, gate_out), (up_send, up_out))[m]
-                held[dst] = (stage[slot] * gain_ref[...]).astype(BF16)
-
-                @pl.when(dst == me)
+                block_f32 = block_f32 * gain_col[...]
+            rounded = block_f32.astype(BF16)
+
+            @pl.when(dst == me)
+            def _():
+                out[me] = rounded
+
+            @pl.when(dst != me)
+            def _():
+                if m == 0:
+                    held[dst] = rounded
+                    block_copy(m, held, out, dst).start()
+                else:
+                    packed[slot] = rounded
+                    store(held, step).start()
+
+            if m > 0:
+
+                @pl.when(jnp.logical_and(step > 0, send_order(step - 1) != me))
                 def _():
-                    pltpu.make_async_copy(held.at[me], out.at[me], keep_sem.at[m]).start()
-
-                @pl.when(dst != me)
-                def _():
-                    block_copy(m, held, out, dst).start()
-            else:
-
-                @pl.when(dst == me)
-                def _():
-                    down_recv[me] = stage[slot].astype(BF16)
-
-                @pl.when(dst != me)
-                def _():
-                    down_send[dst] = stage[slot].astype(BF16)
+                    stored(m, held, out, step - 1)
+
+        def store(held, step):
+            slot = lax.rem(m * fs_count + step, 2)
+            return pltpu.make_async_copy(
+                packed.at[slot], held.at[send_order(step)], store_sem.at[slot]
+            )
+
+        def stored(m, held, out, step):
+            store(held, step).wait()
+            if m == 1:
+                block_copy(m, held, out, send_order(step)).start()
 
         loop(fs_count, body)
+        if m > 0:
+            held, out = ((up_send, up_out), (down_send, down_out))[m - 1]
+
+            @pl.when(send_order(fs_count - 1) != me)
+            def _():
+                stored(m, held, out, fs_count - 1)
 
     convert(0, gate_hbm, up_hbm)
 
@@ -194,34 +231,34 @@
 
     convert(1, up_hbm, down_hbm)
     convert(2, down_hbm, None)
-    loop(pieces, lambda p: loop(fs_count - 1, lambda s: piece_copy(p, send_order(s)).start()))
+    def pc(p, s):
+        dst = send_order(s)
+
+        @pl.when(dst != me)
+        def _():
+            piece_copy(p, dst).start()
+
+    loop(pieces, lambda p: loop(fs_count, lambda s: pc(p, s)))
 
     wait_bytes(x_all.at[pl.ds(0, fs_count - 1)], x_sem.at[3])
 
-    def project(m, held, out, a):
-        act[a] = jnp.zeros_like(act[a])
+    def project(m, out):
+        act[m] = jnp.zeros_like(act[m])
 
         def body(k):
             g = jnp.where(k < half, near_source(k), far_source(k - half))
 
-            @pl.when(g == me)
-            def _():
-                wait_bytes(held.at[me], keep_sem.at[m])
-
             @pl.when(g != me)
             def _():
                 wait_bytes(out.at[g], recv_sem.at[m, g])
 
-            fetch = pltpu.make_async_copy(out.at[g], wbuf, wload_sem)
-            fetch.start()
             x = x_all[g].astype(F32).reshape(tokens, width).astype(BF16)
-            fetch.wait()
-            act[a] += jnp.dot(x, wbuf[...], preferred_element_type=F32)
+            act[m] += jnp.dot(x, out[g], preferred_element_type=F32)
 
         loop(fs_count, body)
 
-    project(0, gate_send, gate_out, 0)
-    project(1, up_send, up_out, 1)
+    project(0, gate_out)
+    project(1, up_out)
     gate = act[0]
     hidden[...] = (gate / (1.0 + jnp.exp(-gate)) * act[1]).astype(BF16)
 
@@ -264,13 +301,10 @@
 
             @pl.when(g != me)
             def _():
-                wait_bytes(down_recv.at[g, span], down_sem.at[p, g])
-
-            pltpu.make_async_copy(
-                down_recv.at[g, span], down_out.at[g, span], down_keep
-            ).start()
+                wait_bytes(down_out.at[g, span], down_sem.at[p, g])
+
             out = lax.dot_general(
-                hidden[...], down_recv[g, span], (((1,), (1,)), ((), ())),
+                hidden[...], down_out[g, span], (((1,), (1,)), ((), ())),
                 preferred_element_type=F32,
             )
             part[r, :, g - base_of(r)] = out.reshape(fs_count, own, rows).astype(BF16)
@@ -296,15 +330,22 @@
         def _():
             finish(r - 1)
 
+    turn[...] = jnp.zeros_like(turn)
+    first, second = logits_ref[0:1], logits_ref[1:2]
+    share_first = 1.0 / (1.0 + jnp.exp(second - first))
+    share_second = 1.0 / (1.0 + jnp.exp(first - second))
+    for e in range(experts):
+        turn[e : e + 1, :own] = jnp.where(routes_ref[0:1] == e, share_first, 0.0) + jnp.where(
+            routes_ref[1:2] == e, share_second, 0.0
+        )
+    weights = turn[...].T
+
     loop(rounds, run_round)
 
     @pl.when(index < fs_count)
     def _():
         finish(rounds - 1)
 
-    first, second = logits_ref[:, 0:1], logits_ref[:, 1:2]
-    share_first = 1.0 / (1.0 + jnp.exp(second - first))
-    share_second = 1.0 / (1.0 + jnp.exp(first - second))
     for p in range(pieces):
         mixed = [jnp.zeros((own, rows), F32)] * share
         for e in range(experts):
@@ -313,16 +354,12 @@
             def _(e=e, p=p):
                 wait_bytes(home.at[e, p], home_recv.at[p, e])
 
-            weight = jnp.where(routes_ref[:, 0:1] == e, share_first, 0.0) + jnp.where(
-                routes_ref[:, 1:2] == e, share_second, 0.0
-            )
             for j in range(share):
-                mixed[j] = mixed[j] + weight * home[e, p, j].astype(F32)
+                mixed[j] = mixed[j] + weights[:own, e : e + 1] * home[e, p, j].astype(F32)
         for j in range(share):
             column = j * width + p * rows
             mixed_out[:, column : column + rows] = mixed[j].astype(BF16)
 
-    wait_bytes(down_recv, down_keep)
     wait_bytes(xcol.at[pl.ds(0, fs_count - 1)], x_sem.at[0])
     wait_bytes(x_all.at[pl.ds(0, fs_count - 1)], x_sem.at[2])
     for m, held in enumerate((gate_send, up_send, down_send)):
@@ -360,19 +397,20 @@
     dma = pltpu.SemaphoreType.DMA
     vmem = pl.BlockSpec(memory_space=pltpu.VMEM)
     anywhere = pl.BlockSpec(memory_space=pl.ANY)
-    landed = jax.ShapeDtypeStruct((fs_count, width, block), BF16)
-    mixed, *landings = pl.pallas_call(
+    pinned = [pltpu.VMEM((own, model // tp_count), BF16)]
+    pinned += [pltpu.VMEM((fs_count, width, block), BF16)] * 3
+    spare = [jax.ShapeDtypeStruct((fs_count, width, block), BF16)] * 2
+    outs = pl.pallas_call(
         functools.partial(fused_kernel, fs_count, tp_count, experts, pieces),
         in_specs=[vmem] * 4 + [anywhere] * 3,
-        out_specs=[vmem] + [anywhere] * 3,
-        out_shape=[jax.ShapeDtypeStruct((own, model // tp_count), BF16)] + [landed] * 3,
+        out_specs=[vmem] * 4 + [anywhere] * 2,
+        out_shape=pinned + spare,
         scratch_shapes=[
             pltpu.VMEM((2, width, block), F32),
             pltpu.VMEM((fs_count, width, block), BF16),
-            pltpu.VMEM((fs_count, width, block), BF16),
-            pltpu.VMEM((fs_count, width, block), BF16),
-            pltpu.VMEM((fs_count, width, block), BF16),
-            pltpu.VMEM((width, block), BF16),
+            pltpu.VMEM((2, width, block), BF16),
+            pltpu.VMEM((8, 128), F32),
+            pltpu.VMEM((width, 1), F32),
             pltpu.VMEM((share, own, width), BF16),
             pltpu.VMEM((fs_count, own, width), BF16),
             pltpu.VMEM((fs_count, fs_count, own, width), BF16),
@@ -382,16 +420,25 @@
             pltpu.VMEM((rounds, group - 1, half, own, rows), BF16),
             pltpu.VMEM((rounds, half, own, rows), BF16),
             pltpu.VMEM((experts, pieces, share, own, rows), BF16),
-            dma((2,)), dma((3,)), dma((2, fs_count)), dma((2,)), dma((pieces, fs_count)), dma,
-            dma((4,)), dma, dma((rounds,)), dma((rounds,)), dma((rounds, tp_count // 2)),
+            dma((2,)), dma((2,)), dma((3,)), dma((2, fs_count)), dma((pieces, fs_count)),
+            dma((4,)), dma((rounds,)), dma((rounds,)), dma((rounds, tp_count // 2)),
             dma((pieces, experts)),
         ],
         compiler_params=pltpu.CompilerParams(
-            collective_id=0, has_side_effects=True, vmem_limit_bytes=63 * 1024 * 1024
+            collective_id=0, has_side_effects=True, vmem_limit_bytes=VMEM_BYTES - 6 * fs_count * width * block
         ),
     )(
-        tokens, routes, route_logits, norm_gain[:, None], gate_weight, up_weight, down_weight
+        tokens, routes.T, route_logits.T, norm_gain.reshape(-1, 128),
+        gate_weight, up_weight, down_weight,
     )
+    mixed, *landings = pl.pallas_call(
+        store_kernel,
+        in_specs=[vmem] * 4,
+        out_specs=[anywhere] * 4,
+        out_shape=[jax.ShapeDtypeStruct(x.shape, x.dtype) for x in outs[:4]],
+        scratch_shapes=[dma((4,))],
+        compiler_params=pltpu.CompilerParams(vmem_limit_bytes=4 * 1024 * 1024),
+    )(*outs[:4])
     return (mixed, *(x.reshape(1, fs_count * width, block) for x in landings))
 
 

time: 622 us -> 581 us (0.934)
  local copies, waits for them, and re-layouts: 29.1 us -> 0 us
  Pallas kernels: 591 us -> 580 us
    unnamed x6 -> x0, local copies, waits for them, and re-layouts: 27.5 us -> none
    pallas_call x1, Pallas kernels: 591 us -> 572 us  [per_device(): pl.pallas_call(functools.partial(fused_kernel, fs_count, tp_count, expert...]
    pallas_call x0 -> x1, Pallas kernels: none -> 8.4 us  [per_device(): pl.pallas_call(store_kernel, in_specs=[vmem] * 4, out_specs=[anywhere] *...]
where the time goes in v2:
time: 581 us
  Pallas kernels  580 us (100%)
    pallas_call x1, Pallas kernels, per_device(): pl.pallas_call(functools.partial(fused_kernel, fs_count, tp_count, expert...  572 us

profile of v2, /device:TPU:0, one launch (start us, length us, event | category | flops | bytes accessed | tf_op | source)
XLA Modules:
  0.0 580.7 jit_solution(11791580195159504309)
XLA Ops:
  0.6 571.6 %shard_map.102 = (bf16[40,1024]{1,0:T(8,128)(2,1)S(1)}, bf16[8,512,1024]{2,1,0:T(8,128)(2,1)S(1)}, bf16[8,512,1024]{2,1,0:T(8,128)(2,1)S(1)}, bf16[8,512,1024]{2...) custom-call(bf16[40,4096]{1,0:T(8,128)(2,1)} %tok_ref.1, s32[2,40]{1,0:T(2,128)} %bitcast.7, ...), custom_call_target="tpu_custom_call" | custom-call | tf_op jit(solution)/shard_map/pallas_call | solution.py:403
  572.3 8.4 %shard_map.103 = (bf16[40,1024]{1,0:T(8,128)(2,1)}, bf16[8,512,1024]{2,1,0:T(8,128)(2,1)}, bf16[8,512,1024]{2,1,0:T(8,128)(2,1)}, bf16[8,512,1024]{2,1,0:T(8,128)(2,1)}) custom-call(bf16[40,1024]{1,0:T(8,128)(2,1)S(1)} %get-tuple-element.12.refs_0_, bf16[8,512,1024]{2,1,0:T(8,128)(2,1)S(1)} %get-tuple-element.13.refs_1_, ...), custom_call_target="tpu_custom_call" | custom-call | tf_op jit(solution)/shard_map/pallas_call | solution.py:434

commit v3 on v2

--- a/solution.py
+++ b/solution.py
@@ -36,13 +36,13 @@
 
 
 def fused_kernel(
-    fs_count, tp_count, experts, pieces,
+    fs_count, tp_count, experts, pieces, relayed,
     tok_ref, routes_ref, logits_ref, gain_ref, gate_hbm, up_hbm, down_hbm,
     mixed_out, gate_out, up_out, down_out, up_send, down_send,
     stage, gate_send, packed, turn, gain_col,
-    xown, xcol, x_all, act, hidden, part, rs_recv, total, home,
+    xown, xcol, x_all, act, hidden, part, rs_recv, total, home, relay, shares,
     load_sem, store_sem, send_sem, recv_sem, down_sem, x_sem,
-    rs_send_sem, rs_recv_sem, home_send, home_recv,
+    rs_send_sem, rs_recv_sem, home_send, home_recv, relay_send, relay_recv, share_sem,
 ):
     me, my_tp = lax.axis_index("fs"), lax.axis_index("tp")
     spread = fs_count // experts
@@ -59,6 +59,17 @@
     pairs = tp_count // 2
     rounds = 2 * pieces
     owner_fs, owner_tp = me // tp_count, lax.rem(me, tp_count)
+    depth = experts // 2 - 1
+    bridge = jnp.where(side == 0, depth, experts - 1 - depth)
+    far_bridge = experts - 1 - bridge
+    at_bridge = mine == bridge
+    far_home = index // half != side
+    home[...] = jnp.zeros_like(home)
+    near_slots = pl.ds(0, half - 1)
+    far_slots = pl.ds((1 - side) * half, half)
+
+    def ranked(k):
+        return jnp.where(side == 0, k, experts - 1 - k)
 
     def send_order(step):
         return lax.rem(me + half + step, fs_count)
@@ -130,15 +141,43 @@
     homes = jnp.where(index < fs_count, tp_count, 0) - jnp.where(index == me, 1, 0)
     pl.semaphore_wait(barrier, fs_count + group - 2 + homes)
 
-    def x_send(s):
-        dst = lax.rem(me + 1 + s, fs_count)
+    def x_send(dst):
         pltpu.make_async_remote_copy(
             src_ref=xown.at[lax.rem(lax.rem(dst, spread), share)], dst_ref=xcol.at[me],
             send_sem=x_sem.at[0], recv_sem=x_sem.at[1], device_id={"fs": dst},
             device_id_type=MESH,
         ).start()
 
-    loop(fs_count - 1, x_send)
+    loop(spread, lambda h: x_send(far_bridge * spread + lax.rem(inner + h, spread)))
+    loop(half - 1, lambda s: x_send(side * half + lax.rem(me + 1 + s, half)))
+
+    def shares_copy(fs):
+        return pltpu.make_async_remote_copy(
+            src_ref=turn, dst_ref=shares, send_sem=share_sem.at[0], recv_sem=share_sem.at[1],
+            device_id={"fs": fs}, device_id_type=MESH,
+        )
+
+    def for_planes(action):
+        for e in range(experts):
+            fs = e * spread + owner_fs
+
+            @pl.when(jnp.logical_and(my_tp == owner_tp, fs != me))
+            def _(fs=fs):
+                action(fs)
+
+    turn[...] = jnp.zeros_like(turn)
+    first, second = logits_ref[0:1], logits_ref[1:2]
+    share_first = 1.0 / (1.0 + jnp.exp(second - first))
+    share_second = 1.0 / (1.0 + jnp.exp(first - second))
+    for e in range(experts):
+        turn[e : e + 1, :own] = jnp.where(routes_ref[0:1] == e, share_first, 0.0) + jnp.where(
+            routes_ref[1:2] == e, share_second, 0.0
+        )
+    for_planes(lambda fs: shares_copy(fs).start())
+
+    @pl.when(index == me)
+    def _():
+        shares[...] = turn[...]
 
     def block_copy(m, held, out, dst):
         return pltpu.make_async_remote_copy(
@@ -216,7 +255,23 @@
 
     convert(0, gate_hbm, up_hbm)
 
-    wait_bytes(xcol.at[pl.ds(0, fs_count - 1)], x_sem.at[1])
+    def x_forward(k):
+        return pltpu.make_async_remote_copy(
+            src_ref=xcol.at[far_slots], dst_ref=xcol.at[far_slots], send_sem=x_sem.at[4],
+            recv_sem=x_sem.at[5], device_id={"fs": ranked(k) * spread + inner},
+            device_id_type=MESH,
+        )
+
+    @pl.when(at_bridge)
+    def _():
+        wait_bytes(xcol.at[pl.ds(0, fs_count - 1)], x_sem.at[1])
+        loop(depth, lambda k: x_forward(k).start())
+
+    @pl.when(jnp.logical_not(at_bridge))
+    def _():
+        wait_bytes(xcol.at[near_slots], x_sem.at[1])
+        wait_bytes(xcol.at[far_slots], x_sem.at[5])
+
     held_part = my_tp * share + lax.rem(inner, share)
 
     def x_gather(s):
@@ -266,14 +321,49 @@
         return jnp.where(lax.rem(r, 2) == 0, side, 1 - side) * half
 
     def finish(r):
-        p = r // 2
         wait_bytes(rs_recv.at[r], rs_recv_sem.at[r])
 
         def add(s, acc):
             return acc + rs_recv[r, s].astype(F32)
 
         acc = lax.fori_loop(0, group - 1, add, part[r, index].astype(F32))
+        columns = shares[...].T
+        lanes = lax.broadcasted_iota(jnp.int32, columns.shape, 1)
+        scale = jnp.sum(jnp.where(lanes == mine, columns, 0.0), axis=1, keepdims=True)
+        total[r] = (acc * scale[:own][None]).astype(BF16)
+        if relayed == 0:
+            send_home(r)
+            return
+        detour = detours(r)
+
+        @pl.when(jnp.logical_and(detour, jnp.logical_not(at_bridge)))
+        def _():
+            relay_copy(r).start()
+
+        @pl.when(jnp.logical_not(detour))
+        def _():
+            send_home(r)
+
+    def detours(r):
+        return jnp.logical_and(far_home, r < relayed)
+
+    def relay_copy(r):
+        return pltpu.make_async_remote_copy(
+            src_ref=total.at[r], dst_ref=relay.at[r, jnp.where(side == 0, mine, experts - 1 - mine)],
+            send_sem=relay_send.at[r], recv_sem=relay_recv.at[r],
+            device_id={"fs": bridge * spread + inner}, device_id_type=MESH,
+        )
+
+    def cross(r):
+        wait_bytes(relay.at[r], relay_recv.at[r])
+        acc = total[r].astype(F32)
+        for k in range(depth):
+            acc = acc + relay[r, k].astype(F32)
         total[r] = acc.astype(BF16)
+        send_home(r)
+
+    def send_home(r):
+        p = r // 2
         for q in range(pairs):
             tp = base_of(r) // share + q
 
@@ -330,37 +420,51 @@
         def _():
             finish(r - 1)
 
-    turn[...] = jnp.zeros_like(turn)
-    first, second = logits_ref[0:1], logits_ref[1:2]
-    share_first = 1.0 / (1.0 + jnp.exp(second - first))
-    share_second = 1.0 / (1.0 + jnp.exp(first - second))
-    for e in range(experts):
-        turn[e : e + 1, :own] = jnp.where(routes_ref[0:1] == e, share_first, 0.0) + jnp.where(
-            routes_ref[1:2] == e, share_second, 0.0
-        )
-    weights = turn[...].T
+    @pl.when(jnp.logical_and(index < fs_count, index != me))
+    def _():
+        wait_bytes(shares, share_sem.at[1])
 
     loop(rounds, run_round)
 
     @pl.when(index < fs_count)
     def _():
+        if relayed > 0:
+
+            @pl.when(jnp.logical_and(far_home, at_bridge))
+            def _():
+                loop(relayed, cross)
+
         finish(rounds - 1)
 
     for p in range(pieces):
         mixed = [jnp.zeros((own, rows), F32)] * share
         for e in range(experts):
 
-            @pl.when(jnp.logical_not(is_self(*sender_of(e))))
+            sent = jnp.logical_not(is_self(*sender_of(e)))
+            if relayed > 0:
+                apart = jnp.where(my_tp // pairs == e // (depth + 1), 0, 1)
+                skipped = jnp.logical_and(side != e // (depth + 1), 2 * p + apart < relayed)
+                sent = jnp.logical_and(
+                    sent, jnp.logical_or(jnp.logical_not(skipped), e == far_bridge)
+                )
+
+            @pl.when(sent)
             def _(e=e, p=p):
                 wait_bytes(home.at[e, p], home_recv.at[p, e])
 
             for j in range(share):
-                mixed[j] = mixed[j] + weights[:own, e : e + 1] * home[e, p, j].astype(F32)
+                mixed[j] = mixed[j] + home[e, p, j].astype(F32)
         for j in range(share):
             column = j * width + p * rows
             mixed_out[:, column : column + rows] = mixed[j].astype(BF16)
 
-    wait_bytes(xcol.at[pl.ds(0, fs_count - 1)], x_sem.at[0])
+    wait_bytes(xcol.at[pl.ds(0, spread + half - 1)], x_sem.at[0])
+    for_planes(lambda fs: shares_copy(fs).wait_send())
+
+    @pl.when(at_bridge)
+    def _():
+        loop(depth, lambda k: x_forward(k).wait_send())
+
     wait_bytes(x_all.at[pl.ds(0, fs_count - 1)], x_sem.at[2])
     for m, held in enumerate((gate_send, up_send, down_send)):
         wait_bytes(held.at[pl.ds(0, fs_count - 1)], send_sem.at[m])
@@ -369,10 +473,16 @@
         @pl.when(index < fs_count)
         def _():
             wait_bytes(part.at[r, pl.ds(0, fs_count - 1)], rs_send_sem.at[r])
+            passed = jnp.logical_and(detours(r), jnp.logical_not(at_bridge))
+
+            @pl.when(passed)
+            def _():
+                relay_copy(r).wait_send()
+
             for q in range(pairs):
                 tp = base_of(r) // share + q
 
-                @pl.when(jnp.logical_not(is_self(index, tp)))
+                @pl.when(jnp.logical_not(jnp.logical_or(passed, is_self(index, tp))))
                 def _(q=q):
                     wait_bytes(total.at[r, pl.ds(q * share, share)], home_send.at[r, q])
 
@@ -394,6 +504,8 @@
     pieces = max(1, width // 128)
     rows = width // pieces
     rounds = 2 * pieces
+    relayed = max(0, rounds - 2)
+    depth = max(1, experts // 2 - 1)
     dma = pltpu.SemaphoreType.DMA
     vmem = pl.BlockSpec(memory_space=pltpu.VMEM)
     anywhere = pl.BlockSpec(memory_space=pl.ANY)
@@ -401,7 +513,7 @@
     pinned += [pltpu.VMEM((fs_count, width, block), BF16)] * 3
     spare = [jax.ShapeDtypeStruct((fs_count, width, block), BF16)] * 2
     outs = pl.pallas_call(
-        functools.partial(fused_kernel, fs_count, tp_count, experts, pieces),
+        functools.partial(fused_kernel, fs_count, tp_count, experts, pieces, relayed),
         in_specs=[vmem] * 4 + [anywhere] * 3,
         out_specs=[vmem] * 4 + [anywhere] * 2,
         out_shape=pinned + spare,
@@ -420,9 +532,11 @@
             pltpu.VMEM((rounds, group - 1, half, own, rows), BF16),
             pltpu.VMEM((rounds, half, own, rows), BF16),
             pltpu.VMEM((experts, pieces, share, own, rows), BF16),
+            pltpu.VMEM((max(1, relayed), depth, half, own, rows), BF16),
+            pltpu.VMEM((8, 128), F32),
             dma((2,)), dma((2,)), dma((3,)), dma((2, fs_count)), dma((pieces, fs_count)),
-            dma((4,)), dma((rounds,)), dma((rounds,)), dma((rounds, tp_count // 2)),
-            dma((pieces, experts)),
+            dma((6,)), dma((rounds,)), dma((rounds,)), dma((rounds, tp_count // 2)),
+            dma((pieces, experts)), dma((max(1, relayed),)), dma((max(1, relayed),)), dma((2,)),
         ],
         compiler_params=pltpu.CompilerParams(
             collective_id=0, has_side_effects=True, vmem_limit_bytes=VMEM_BYTES - 6 * fs_count * width * block

time: 581 us -> 573 us (0.986)
  Pallas kernels: 580 us -> 572 us
    pallas_call x1, Pallas kernels: 572 us -> 563 us  [per_device(): pl.pallas_call(functools.partial(fused_kernel, fs_count, tp_count, expert...]
where the time goes in v3:
time: 573 us; the launch traced here: 572 us
  Pallas kernels  572 us (100%)
    pallas_call x1, Pallas kernels, per_device(): pl.pallas_call(functools.partial(fused_kernel, fs_count, tp_count, expert...  563 us

profile of v3, /device:TPU:0, one launch (start us, length us, event | category | flops | bytes accessed | tf_op | source)
XLA Modules:
  0.0 572.3 jit_solution(6738396798564508988)
XLA Ops:
  0.6 563.2 %shard_map.102 = (bf16[40,1024]{1,0:T(8,128)(2,1)S(1)}, bf16[8,512,1024]{2,1,0:T(8,128)(2,1)S(1)}, bf16[8,512,1024]{2,1,0:T(8,128)(2,1)S(1)}, bf16[8,512,1024]{2...) custom-call(bf16[40,4096]{1,0:T(8,128)(2,1)} %tok_ref.1, s32[2,40]{1,0:T(2,128)} %bitcast.7, ...), custom_call_target="tpu_custom_call" | custom-call | tf_op jit(solution)/shard_map/pallas_call | solution.py:515
  563.9 8.4 %shard_map.103 = (bf16[40,1024]{1,0:T(8,128)(2,1)}, bf16[8,512,1024]{2,1,0:T(8,128)(2,1)}, bf16[8,512,1024]{2,1,0:T(8,128)(2,1)}, bf16[8,512,1024]{2,1,0:T(8,128)(2,1)}) custom-call(bf16[40,1024]{1,0:T(8,128)(2,1)S(1)} %get-tuple-element.12.refs_0_, bf16[8,512,1024]{2,1,0:T(8,128)(2,1)S(1)} %get-tuple-element.13.refs_1_, ...), custom_call_target="tpu_custom_call" | custom-call | tf_op jit(solution)/shard_map/pallas_call | solution.py:548

commit v4 on v3

--- a/solution.py
+++ b/solution.py
@@ -37,12 +37,13 @@
 
 def fused_kernel(
     fs_count, tp_count, experts, pieces, relayed,
-    tok_ref, routes_ref, logits_ref, gain_ref, gate_hbm, up_hbm, down_hbm,
+    tok_hbm, routes_hbm, logits_hbm, gain_hbm, gate_hbm, up_hbm, down_hbm,
     mixed_out, gate_out, up_out, down_out, up_send, down_send,
-    stage, gate_send, packed, turn, gain_col,
+    tok_ref, routes_ref, logits_ref, gain_ref, stage, gate_send, packed, turn, gain_col,
+    share_col,
     xown, xcol, x_all, act, hidden, part, rs_recv, total, home, relay, shares,
     load_sem, store_sem, send_sem, recv_sem, down_sem, x_sem,
-    rs_send_sem, rs_recv_sem, home_send, home_recv, relay_send, relay_recv, share_sem,
+    rs_send_sem, rs_recv_sem, home_send, home_recv, relay_send, relay_recv, share_sem, small_sem,
 ):
     me, my_tp = lax.axis_index("fs"), lax.axis_index("tp")
     spread = fs_count // experts
@@ -58,13 +59,19 @@
     tokens = fs_count * own
     pairs = tp_count // 2
     rounds = 2 * pieces
-    owner_fs, owner_tp = me // tp_count, lax.rem(me, tp_count)
+    planes = experts // 2
+
+    def seat(z):
+        return lax.rem(z, planes) * 2 + z // planes
+
+    handled = (lax.rem(my_tp, 2) * planes + my_tp // 2) * spread + inner
+    handles = my_tp < experts
+    own_home = jnp.logical_and(handles, handled == me)
     depth = experts // 2 - 1
     bridge = jnp.where(side == 0, depth, experts - 1 - depth)
     far_bridge = experts - 1 - bridge
     at_bridge = mine == bridge
-    far_home = index // half != side
-    home[...] = jnp.zeros_like(home)
+    far_home = handled // half != side
     near_slots = pl.ds(0, half - 1)
     far_slots = pl.ds((1 - side) * half, half)
 
@@ -86,8 +93,17 @@
         return fs, other // share
 
     def plane_peer(i):
-        return mine * spread + i // tp_count, lax.rem(i, tp_count)
-
+        return mine * spread + lax.rem(i, spread), seat(i // spread)
+
+    small = [
+        pltpu.make_async_copy(hbm, ref, small_sem.at[i])
+        for i, (hbm, ref) in enumerate(
+            (
+                (gain_hbm, gain_ref), (tok_hbm, tok_ref), (routes_hbm, routes_ref),
+                (logits_hbm, logits_ref),
+            )
+        )
+    ]
     barrier = pltpu.get_barrier_semaphore()
 
     def signal(fs, tp):
@@ -102,17 +118,21 @@
             hbm.at[dst // spread, :, pl.ds(column, block)], stage.at[slot], load_sem.at[slot]
         )
 
+    small[0].start()
     load(gate_hbm, 0, 0).start()
+    for copy in small[1:]:
+        copy.start()
+    home[...] = jnp.zeros_like(home)
     loop(fs_count - 1, lambda s: signal(lax.rem(me + 1 + s, fs_count), my_tp))
 
     def greet(s):
-        fs, tp = plane_peer(lax.rem(index + 1 + s, group))
-        signal(fs, tp)
+        other = lax.rem(index + 1 + s, group)
+        signal(mine * spread + other // tp_count, lax.rem(other, tp_count))
 
     loop(group - 1, greet)
 
     def sender_of(e):
-        return e * spread + owner_fs, owner_tp
+        return e * spread + inner, seat(mine)
 
     def is_self(fs, tp):
         return jnp.logical_and(fs == me, tp == my_tp)
@@ -125,11 +145,17 @@
             signal(fs, tp)
 
     turn[...] = jnp.zeros_like(turn)
+    small[0].wait()
     turn[: gain_ref.shape[0]] = gain_ref[...]
     turned = turn[...].T
     for q in range(width // 128):
         gain_col[q * 128 : (q + 1) * 128] = turned[:, q : q + 1]
 
+    load(gate_hbm, 0, 0).wait()
+    load(gate_hbm, 1, 1).start()
+    gate_send[send_order(0)] = (stage[0] * gain_col[...]).astype(BF16)
+    for copy in small[1:]:
+        copy.wait()
     tok = tok_ref[...].astype(F32)
     scale = lax.rsqrt(jnp.mean(tok * tok, axis=1, keepdims=True) + 1e-05)
     for j in range(share):
@@ -138,8 +164,16 @@
         xown[j] = (cols * scale).astype(BF16)
     xcol[me] = xown[lax.rem(inner, share)]
 
-    homes = jnp.where(index < fs_count, tp_count, 0) - jnp.where(index == me, 1, 0)
+    homes = jnp.where(handles, tp_count, 0) - jnp.where(own_home, 1, 0)
     pl.semaphore_wait(barrier, fs_count + group - 2 + homes)
+
+    def block_copy(m, held, out, dst):
+        return pltpu.make_async_remote_copy(
+            src_ref=held.at[dst], dst_ref=out.at[me], send_sem=send_sem.at[m],
+            recv_sem=recv_sem.at[m, me], device_id={"fs": dst}, device_id_type=MESH,
+        )
+
+    block_copy(0, gate_send, gate_out, send_order(0)).start()
 
     def x_send(dst):
         pltpu.make_async_remote_copy(
@@ -159,9 +193,9 @@
 
     def for_planes(action):
         for e in range(experts):
-            fs = e * spread + owner_fs
-
-            @pl.when(jnp.logical_and(my_tp == owner_tp, fs != me))
+            fs = e * spread + inner
+
+            @pl.when(jnp.logical_and(my_tp == seat(mine), fs != me))
             def _(fs=fs):
                 action(fs)
 
@@ -175,15 +209,9 @@
         )
     for_planes(lambda fs: shares_copy(fs).start())
 
-    @pl.when(index == me)
+    @pl.when(own_home)
     def _():
         shares[...] = turn[...]
-
-    def block_copy(m, held, out, dst):
-        return pltpu.make_async_remote_copy(
-            src_ref=held.at[dst], dst_ref=out.at[me], send_sem=send_sem.at[m],
-            recv_sem=recv_sem.at[m, me], device_id={"fs": dst}, device_id_type=MESH,
-        )
 
     def piece_copy(p, dst):
         span = pl.ds(pl.multiple_of(p * rows, rows), rows)
@@ -194,7 +222,10 @@
         )
 
     def convert(m, hbm, following):
-        def body(step):
+        begin = 1 if m == 0 else 0
+
+        def body(i):
+            step = i + begin
             slot = lax.rem(m * fs_count + step, 2)
             dst = send_order(step)
 
@@ -245,7 +276,7 @@
             if m == 1:
                 block_copy(m, held, out, send_order(step)).start()
 
-        loop(fs_count, body)
+        loop(fs_count - begin, body)
         if m > 0:
             held, out = ((up_send, up_out), (down_send, down_out))[m - 1]
 
@@ -326,11 +357,8 @@
         def add(s, acc):
             return acc + rs_recv[r, s].astype(F32)
 
-        acc = lax.fori_loop(0, group - 1, add, part[r, index].astype(F32))
-        columns = shares[...].T
-        lanes = lax.broadcasted_iota(jnp.int32, columns.shape, 1)
-        scale = jnp.sum(jnp.where(lanes == mine, columns, 0.0), axis=1, keepdims=True)
-        total[r] = (acc * scale[:own][None]).astype(BF16)
+        acc = lax.fori_loop(0, group - 1, add, part[r, handled].astype(F32))
+        total[r] = (acc * share_col[...][None]).astype(BF16)
         if relayed == 0:
             send_home(r)
             return
@@ -367,28 +395,29 @@
         for q in range(pairs):
             tp = base_of(r) // share + q
 
-            @pl.when(is_self(index, tp))
+            @pl.when(is_self(handled, tp))
             def _(q=q):
-                home[mine, p] = total[r, pl.ds(q * share, share)]
-
-            @pl.when(jnp.logical_not(is_self(index, tp)))
+                home[mine, p] = total[r, q]
+
+            @pl.when(jnp.logical_not(is_self(handled, tp)))
             def _(q=q, tp=tp):
                 home_copy(r, q, tp).start()
 
     def home_copy(r, q, tp):
         return pltpu.make_async_remote_copy(
-            src_ref=total.at[r, pl.ds(q * share, share)], dst_ref=home.at[mine, r // 2],
+            src_ref=total.at[r, q], dst_ref=home.at[mine, r // 2],
             send_sem=home_send.at[r, q], recv_sem=home_recv.at[r // 2, mine],
-            device_id={"fs": index, "tp": tp}, device_id_type=MESH,
-        )
+            device_id={"fs": handled, "tp": tp}, device_id_type=MESH,
+        )
+
+    column = lax.rem(me, half)
+    first_cut = jnp.where(jnp.logical_or(column < share // 2, column >= half - share // 2), 1, 0)
 
     def run_round(r):
         p = r // 2
         span = pl.ds(pl.multiple_of(p * rows, rows), rows)
 
-        def item(k):
-            g = jnp.where(lax.rem(r, 2) == 0, near_source(k), far_source(k))
-
+        def project_back(g):
             @pl.when(g != me)
             def _():
                 wait_bytes(down_out.at[g, span], down_sem.at[p, g])
@@ -397,36 +426,51 @@
                 hidden[...], down_out[g, span], (((1,), (1,)), ((), ())),
                 preferred_element_type=F32,
             )
-            part[r, :, g - base_of(r)] = out.reshape(fs_count, own, rows).astype(BF16)
-
-        loop(half, item)
-
-        def rs_send(s):
-            i = lax.rem(index + 1 + s, fs_count)
-
-            @pl.when(i != index)
-            def _():
+            return out.reshape(fs_count, own, rows)
+
+        def cut(k):
+            q = lax.rem(k + first_cut, pairs)
+            base = base_of(r) + q * share
+            outs = [project_back(base + j) for j in range(share)]
+            part[r, :, q] = jnp.concatenate(outs, axis=1).astype(BF16)
+
+            def rs_send(s):
+                i = lax.rem(me + 1 + s, fs_count)
                 fs, tp = plane_peer(i)
-                slot = lax.rem(index + 2 * group - i - 1, group)
-                pltpu.make_async_remote_copy(
-                    src_ref=part.at[r, i], dst_ref=rs_recv.at[r, slot],
-                    send_sem=rs_send_sem.at[r], recv_sem=rs_recv_sem.at[r],
-                    device_id={"fs": fs, "tp": tp}, device_id_type=MESH,
-                ).start()
-
-        loop(fs_count, rs_send)
-
-        @pl.when(jnp.logical_and(r > 0, index < fs_count))
+
+                @pl.when(jnp.logical_not(is_self(fs, tp)))
+                def _():
+                    place = lax.rem(i, spread) * tp_count + tp
+                    slot = lax.rem(index + 2 * group - place - 1, group)
+                    pltpu.make_async_remote_copy(
+                        src_ref=part.at[r, i, q], dst_ref=rs_recv.at[r, slot, q],
+                        send_sem=rs_send_sem.at[r], recv_sem=rs_recv_sem.at[r],
+                        device_id={"fs": fs, "tp": tp}, device_id_type=MESH,
+                    ).start()
+
+            loop(fs_count, rs_send)
+
+        loop(pairs, cut)
+
+        @pl.when(jnp.logical_and(r > 0, handles))
         def _():
             finish(r - 1)
 
-    @pl.when(jnp.logical_and(index < fs_count, index != me))
+    @pl.when(jnp.logical_and(handles, handled != me))
     def _():
         wait_bytes(shares, share_sem.at[1])
 
+    @pl.when(handles)
+    def _():
+        columns = shares[...].T
+        lanes = lax.broadcasted_iota(jnp.int32, columns.shape, 1)
+        scale = jnp.sum(jnp.where(lanes == mine, columns, 0.0), axis=1, keepdims=True)
+        for j in range(share):
+            share_col[j * own : (j + 1) * own] = scale[:own]
+
     loop(rounds, run_round)
 
-    @pl.when(index < fs_count)
+    @pl.when(handles)
     def _():
         if relayed > 0:
 
@@ -452,8 +496,9 @@
             def _(e=e, p=p):
                 wait_bytes(home.at[e, p], home_recv.at[p, e])
 
+            landed = home[e, p].astype(F32)
             for j in range(share):
-                mixed[j] = mixed[j] + home[e, p, j].astype(F32)
+                mixed[j] = mixed[j] + landed[j * own : (j + 1) * own]
         for j in range(share):
             column = j * width + p * rows
             mixed_out[:, column : column + rows] = mixed[j].astype(BF16)
@@ -470,7 +515,7 @@
         wait_bytes(held.at[pl.ds(0, fs_count - 1)], send_sem.at[m])
 
     def drain(r):
-        @pl.when(index < fs_count)
+        @pl.when(handles)
         def _():
             wait_bytes(part.at[r, pl.ds(0, fs_count - 1)], rs_send_sem.at[r])
             passed = jnp.logical_and(detours(r), jnp.logical_not(at_bridge))
@@ -482,11 +527,11 @@
             for q in range(pairs):
                 tp = base_of(r) // share + q
 
-                @pl.when(jnp.logical_not(jnp.logical_or(passed, is_self(index, tp))))
+                @pl.when(jnp.logical_not(jnp.logical_or(passed, is_self(handled, tp))))
                 def _(q=q):
-                    wait_bytes(total.at[r, pl.ds(q * share, share)], home_send.at[r, q])
-
-        @pl.when(index >= fs_count)
+                    wait_bytes(total.at[r, q], home_send.at[r, q])
+
+        @pl.when(jnp.logical_not(handles))
         def _():
             wait_bytes(part.at[r], rs_send_sem.at[r])
 
@@ -500,7 +545,7 @@
     block = columns // spread
     own, model = tokens.shape
     group = spread * tp_count
-    half, share = fs_count // 2, fs_count // tp_count
+    pairs, share = tp_count // 2, fs_count // tp_count
     pieces = max(1, width // 128)
     rows = width // pieces
     rounds = 2 * pieces
@@ -514,29 +559,35 @@
     spare = [jax.ShapeDtypeStruct((fs_count, width, block), BF16)] * 2
     outs = pl.pallas_call(
         functools.partial(fused_kernel, fs_count, tp_count, experts, pieces, relayed),
-        in_specs=[vmem] * 4 + [anywhere] * 3,
+        in_specs=[anywhere] * 7,
         out_specs=[vmem] * 4 + [anywhere] * 2,
         out_shape=pinned + spare,
         scratch_shapes=[
+            pltpu.VMEM((own, model), BF16),
+            pltpu.VMEM((2, own), jnp.int32),
+            pltpu.VMEM((2, own), F32),
+            pltpu.VMEM((width // 128, 128), F32),
             pltpu.VMEM((2, width, block), F32),
             pltpu.VMEM((fs_count, width, block), BF16),
             pltpu.VMEM((2, width, block), BF16),
             pltpu.VMEM((8, 128), F32),
             pltpu.VMEM((width, 1), F32),
+            pltpu.VMEM((share * own, 1), F32),
             pltpu.VMEM((share, own, width), BF16),
             pltpu.VMEM((fs_count, own, width), BF16),
             pltpu.VMEM((fs_count, fs_count, own, width), BF16),
             pltpu.VMEM((2, fs_count * own, block), F32),
             pltpu.VMEM((fs_count * own, block), BF16),
-            pltpu.VMEM((rounds, fs_count, half, own, rows), BF16),
-            pltpu.VMEM((rounds, group - 1, half, own, rows), BF16),
-            pltpu.VMEM((rounds, half, own, rows), BF16),
-            pltpu.VMEM((experts, pieces, share, own, rows), BF16),
-            pltpu.VMEM((max(1, relayed), depth, half, own, rows), BF16),
+            pltpu.VMEM((rounds, fs_count, pairs, share * own, rows), BF16),
+            pltpu.VMEM((rounds, group - 1, pairs, share * own, rows), BF16),
+            pltpu.VMEM((rounds, pairs, share * own, rows), BF16),
+            pltpu.VMEM((experts, pieces, share * own, rows), BF16),
+            pltpu.VMEM((max(1, relayed), depth, pairs, share * own, rows), BF16),
             pltpu.VMEM((8, 128), F32),
             dma((2,)), dma((2,)), dma((3,)), dma((2, fs_count)), dma((pieces, fs_count)),
             dma((6,)), dma((rounds,)), dma((rounds,)), dma((rounds, tp_count // 2)),
             dma((pieces, experts)), dma((max(1, relayed),)), dma((max(1, relayed),)), dma((2,)),
+            dma((4,)),
         ],
         compiler_params=pltpu.CompilerParams(
             collective_id=0, has_side_effects=True, vmem_limit_bytes=VMEM_BYTES - 6 * fs_count * width * block

time: 573 us -> 571 us (level)
  no operation moved by 1% of the time
where the time goes in v4:
time: 571 us
  Pallas kernels  570 us (100%)
    pallas_call x1, Pallas kernels, per_device(): pl.pallas_call(functools.partial(fused_kernel, fs_count, tp_count, expert...  562 us

profile of v4, /device:TPU:0, one launch (start us, length us, event | category | flops | bytes accessed | tf_op | source)
XLA Modules:
  0.0 570.9 jit_solution(14298573792822075381)
XLA Ops:
  0.6 561.8 %shard_map.102 = (bf16[40,1024]{1,0:T(8,128)(2,1)S(1)}, bf16[8,512,1024]{2,1,0:T(8,128)(2,1)S(1)}, bf16[8,512,1024]{2,1,0:T(8,128)(2,1)S(1)}, bf16[8,512,1024]{2...) custom-call(bf16[40,4096]{1,0:T(8,128)(2,1)} %tok_hbm.1, s32[2,40]{1,0:T(2,128)} %bitcast.7, ...), custom_call_target="tpu_custom_call" | custom-call | tf_op jit(solution)/shard_map/pallas_call | solution.py:560
  562.5 8.4 %shard_map.103 = (bf16[40,1024]{1,0:T(8,128)(2,1)}, bf16[8,512,1024]{2,1,0:T(8,128)(2,1)}, bf16[8,512,1024]{2,1,0:T(8,128)(2,1)}, bf16[8,512,1024]{2,1,0:T(8,128)(2,1)}) custom-call(bf16[40,1024]{1,0:T(8,128)(2,1)S(1)} %get-tuple-element.12.refs_0_, bf16[8,512,1024]{2,1,0:T(8,128)(2,1)S(1)} %get-tuple-element.13.refs_1_, ...), custom_call_target="tpu_custom_call" | custom-call | tf_op jit(solution)/shard_map/pallas_call | solution.py:599

commit v5 on v4

--- a/solution.py
+++ b/solution.py
@@ -154,6 +154,9 @@
     load(gate_hbm, 0, 0).wait()
     load(gate_hbm, 1, 1).start()
     gate_send[send_order(0)] = (stage[0] * gain_col[...]).astype(BF16)
+    load(gate_hbm, 1, 1).wait()
+    load(gate_hbm, 2, 0).start()
+    gate_send[send_order(1)] = (stage[1] * gain_col[...]).astype(BF16)
     for copy in small[1:]:
         copy.wait()
     tok = tok_ref[...].astype(F32)
@@ -174,6 +177,7 @@
         )
 
     block_copy(0, gate_send, gate_out, send_order(0)).start()
+    block_copy(0, gate_send, gate_out, send_order(1)).start()
 
     def x_send(dst):
         pltpu.make_async_remote_copy(
@@ -222,7 +226,7 @@
         )
 
     def convert(m, hbm, following):
-        begin = 1 if m == 0 else 0
+        begin = 2 if m == 0 else 0
 
         def body(i):
             step = i + begin
@@ -450,6 +454,17 @@
 
             loop(fs_count, rs_send)
 
+        if relayed > 0:
+            crossing = jnp.logical_and(jnp.logical_and(handles, far_home), at_bridge)
+
+            @pl.when(jnp.logical_and(crossing, r == rounds - 2))
+            def _():
+                loop(relayed - 2, cross)
+
+            @pl.when(jnp.logical_and(crossing, r == rounds - 1))
+            def _():
+                loop(2, lambda k: cross(relayed - 2 + k))
+
         loop(pairs, cut)
 
         @pl.when(jnp.logical_and(r > 0, handles))
@@ -472,12 +487,6 @@
 
     @pl.when(handles)
     def _():
-        if relayed > 0:
-
-            @pl.when(jnp.logical_and(far_home, at_bridge))
-            def _():
-                loop(relayed, cross)
-
         finish(rounds - 1)
 
     for p in range(pieces):

time: 571 us -> 572 us (level)
  no operation moved by 1% of the time
where the time goes in v5:
time: 572 us
  Pallas kernels  571 us (100%)
    pallas_call x1, Pallas kernels, per_device(): pl.pallas_call(functools.partial(fused_kernel, fs_count, tp_count, expert...  562 us

profile of v5, /device:TPU:0, one launch (start us, length us, event | category | flops | bytes accessed | tf_op | source)
XLA Modules:
  0.0 571.5 jit_solution(6061669531973053617)
XLA Ops:
  0.6 562.5 %shard_map.102 = (bf16[40,1024]{1,0:T(8,128)(2,1)S(1)}, bf16[8,512,1024]{2,1,0:T(8,128)(2,1)S(1)}, bf16[8,512,1024]{2,1,0:T(8,128)(2,1)S(1)}, bf16[8,512,1024]{2...) custom-call(bf16[40,4096]{1,0:T(8,128)(2,1)} %tok_hbm.1, s32[2,40]{1,0:T(2,128)} %bitcast.7, ...), custom_call_target="tpu_custom_call" | custom-call | tf_op jit(solution)/shard_map/pallas_call | solution.py:569
  563.1 8.4 %shard_map.103 = (bf16[40,1024]{1,0:T(8,128)(2,1)}, bf16[8,512,1024]{2,1,0:T(8,128)(2,1)}, bf16[8,512,1024]{2,1,0:T(8,128)(2,1)}, bf16[8,512,1024]{2,1,0:T(8,128)(2,1)}) custom-call(bf16[40,1024]{1,0:T(8,128)(2,1)S(1)} %get-tuple-element.12.refs_0_, bf16[8,512,1024]{2,1,0:T(8,128)(2,1)S(1)} %get-tuple-element.13.refs_1_, ...), custom_call_target="tpu_custom_call" | custom-call | tf_op jit(solution)/shard_map/pallas_call | solution.py:608
